TPU v7x, 32 devices: a whole 2x2x4 slice. The times are simulated.
32 devices in a mesh: ep: 16 (over z, y, x), tp: 2 (over core).
Axes of the slice: x: 2, y: 2, z: 4, core: 2. Of those that a mesh axis runs over, the one named last changes fastest.
Arguments:
- inputs: bfloat16 [1024, 2048], P('ep'), may hold values from -6 to 6
- cache_keys: bfloat16 [1024, 2, 64, 1024], P('ep', 'tp'), may hold values from -6 to 6
- cache_values: bfloat16 [1024, 2, 64, 1024], P('ep', 'tp'), may hold values from -12 to 12
- lengths: int32 [1024], P('ep'), may hold values from 1 to 1024, as said below
- query_weight: bfloat16 [2048, 1024], P(None, 'tp'), may hold values from -0.125 to 0.125
- key_weight: bfloat16 [2048, 128], P(None, 'tp'), may hold values from -0.125 to 0.125
- value_weight: bfloat16 [2048, 128], P(None, 'tp'), may hold values from -0.125 to 0.125
- head_bias: float32 [16], P('tp'), may hold values from -7 to -3
- out_weight: bfloat16 [1024, 2048], P('tp'), may hold values from -0.75 to 0.75
- attend_gain: float32 [2048], replicated, may hold values from 0.1 to 1.9
- router_weight: bfloat16 [2048, 16], replicated, may hold values from -0.125 to 0.125
- routes: int32 [1024, 4], P('ep'), may hold values from 0 to 15, all different within a row; in each aligned block of 64 rows (0 to 63, 64 to 127, ...) at most 32 rows name the same one
- expert_gate: bfloat16 [16, 2048, 512], P('ep', None, 'tp'), may hold values from -0.125 to 0.125
- expert_up: bfloat16 [16, 2048, 512], P('ep', None, 'tp'), may hold values from -0.125 to 0.125
- expert_down: bfloat16 [16, 512, 2048], P('ep', 'tp'), may hold values from -0.25 to 0.25
- shared_gate: bfloat16 [2048, 512], P(None, 'tp'), may hold values from -0.125 to 0.125
- shared_up: bfloat16 [2048, 512], P(None, 'tp'), may hold values from -0.125 to 0.125
- shared_down: bfloat16 [512, 2048], P('tp'), may hold values from -0.25 to 0.25
- final_gain: float32 [2048], P('tp'), may hold values from 0.1 to 1.9
Outputs:
- output: bfloat16 [1024, 2048], P('ep', 'tp')
- new_keys: bfloat16 [1024, 128], P('ep', 'tp')
- new_values: bfloat16 [1024, 128], P('ep', 'tp')
Inputs may be any that keep to these rules, and one draw needn't show every extreme that they name: `lengths`: some sequence has 1024 filled positions and some other has 1. `routes`: each row names 4 different experts. Among the 64 rows of one index of ep no expert is named more than 32 times; some expert is named exactly 32 times by the rows of some index.
All inputs are finite; a program needn't handle non-finite values.
Results may differ from a plain program's by a relative error of at most 0.015.
Values may be sent and summed in bfloat16 or wider, within the bound.
A program may use at most 128 MiB of HBM per device.

v0:
```python
import math

import jax
import jax.numpy as jnp
from jax import lax
from jax.sharding import PartitionSpec as P

RESIDUAL_SCALE = 2.0**0.25
ROUTE_SCALE = 2.5
NORM_EPS = 1e-05


def layer_norm(values, gain_vec):
    row_mean = jnp.mean(values, axis=-1, keepdims=True)
    centered = values - row_mean
    row_var = jnp.mean(centered * centered, axis=-1, keepdims=True)
    return centered * lax.rsqrt(row_var + NORM_EPS) * gain_vec


def strictly_later(size):
    row_pos = lax.broadcasted_iota(jnp.int32, (size, size), 0)
    col_pos = lax.broadcasted_iota(jnp.int32, (size, size), 1)
    return (row_pos > col_pos).astype(jnp.float32)


def later_totals(log_keep):
    lead = log_keep.shape[:-1]
    length = log_keep.shape[-1]
    block_size = math.gcd(length, 128)
    block_count = length // block_size
    blocked = log_keep.reshape(lead + (block_count, block_size))
    inside = jnp.einsum(
        "...bi,ic->...bc", blocked, strictly_later(block_size), precision=lax.Precision.HIGHEST
    )
    block_total = jnp.sum(blocked, axis=-1)
    after = jnp.einsum(
        "...i,ic->...c", block_total, strictly_later(block_count), precision=lax.Precision.HIGHEST
    )
    return (inside + after[..., None]).reshape(lead + (length,))


def on_device(
    inputs,
    cache_keys,
    cache_values,
    lengths,
    query_weight,
    key_weight,
    value_weight,
    head_bias,
    out_weight,
    attend_gain,
    router_weight,
    routes,
    expert_gate,
    expert_up,
    expert_down,
    shared_gate,
    shared_up,
    shared_down,
    final_gain,
):
    seq_count, model_width = inputs.shape
    key_heads, head_size, cache_length = cache_keys.shape[1:]
    query_heads = head_bias.shape[0]
    groups = query_heads // key_heads
    choices_count = routes.shape[1]
    experts = router_weight.shape[1]
    core_index = lax.axis_index("tp")
    half_width = model_width // lax.axis_size("tp")
    query = jnp.dot(inputs, query_weight, preferred_element_type=jnp.float32).astype(jnp.bfloat16)
    query = query.reshape(seq_count, key_heads, groups, head_size)
    new_keys = jnp.dot(inputs, key_weight, preferred_element_type=jnp.float32).astype(jnp.bfloat16)
    new_values = jnp.dot(inputs, value_weight, preferred_element_type=jnp.float32).astype(
        jnp.bfloat16
    )
    scores = jnp.einsum("skgd,skdc->skgc", query, cache_keys, preferred_element_type=jnp.float32)
    scores = scores * head_size ** (-0.5) + head_bias.reshape(key_heads, groups)[None, :, :, None]
    usable = (
        lax.broadcasted_iota(jnp.int32, (1, 1, 1, cache_length), 3) < lengths[:, None, None, None]
    )
    log_keep = jnp.where(usable, jax.nn.log_sigmoid(-scores), 0.0)
    later_sum = later_totals(log_keep)
    stick_weight = jnp.where(usable, jnp.exp(jax.nn.log_sigmoid(scores) + later_sum), 0.0).astype(
        jnp.bfloat16
    )
    attended = jnp.einsum(
        "skgc,skdc->skgd", stick_weight, cache_values, preferred_element_type=jnp.float32
    )
    attended = attended.astype(jnp.bfloat16).reshape(seq_count, query_heads * head_size)
    attention = lax.psum(
        jnp.dot(attended, out_weight, preferred_element_type=jnp.float32).astype(jnp.bfloat16), "tp"
    ).astype(jnp.float32)
    hidden = layer_norm(
        RESIDUAL_SCALE * inputs.astype(jnp.float32) + attention, attend_gain
    ).astype(jnp.bfloat16)
    router_probs = jax.nn.sigmoid(
        jnp.dot(hidden, router_weight, preferred_element_type=jnp.float32)
    )
    picked = routes[:, :, None] == lax.broadcasted_iota(jnp.int32, (1, 1, experts), 2)
    chosen = jnp.sum(jnp.where(picked, router_probs[:, None, :], 0.0), axis=2)
    route_weights = ROUTE_SCALE * chosen / jnp.sum(chosen, axis=1, keepdims=True)
    capacity = 2 * seq_count * choices_count // experts
    row_total = seq_count * choices_count
    onehot_float = picked.reshape(row_total, experts).astype(jnp.float32)
    earlier_count = jnp.dot(
        strictly_later(row_total), onehot_float, precision=lax.Precision.HIGHEST
    )
    slot_index = jnp.sum(earlier_count * onehot_float, axis=1).astype(jnp.int32)
    target = routes.reshape(-1) * capacity + slot_index
    selector_float = (
        target[:, None] == lax.broadcasted_iota(jnp.int32, (1, experts * capacity), 1)
    ).astype(jnp.float32)
    selector = selector_float.astype(jnp.bfloat16)
    placement = jnp.sum(selector_float.reshape(seq_count, choices_count, -1), axis=1).astype(
        jnp.bfloat16
    )
    outgoing = lax.dot_general(
        placement, hidden, (((0,), (0,)), ((), ())), preferred_element_type=jnp.float32
    )
    outgoing = outgoing.astype(jnp.bfloat16).reshape(experts, capacity, -1)
    arrived = lax.all_to_all(outgoing, "ep", split_axis=0, concat_axis=0, tiled=True)
    senders, slot_count, _ = arrived.shape
    flat_rows = arrived.reshape(senders * slot_count, -1)
    gate_act = jnp.dot(flat_rows, expert_gate[0], preferred_element_type=jnp.float32)
    up_act = jnp.dot(flat_rows, expert_up[0], preferred_element_type=jnp.float32)
    inner = (jax.nn.silu(gate_act) * up_act).astype(jnp.bfloat16)
    partial_value = jnp.dot(inner, expert_down[0], preferred_element_type=jnp.float32)
    summed = lax.psum_scatter(
        partial_value.astype(jnp.bfloat16), "tp", scatter_dimension=1, tiled=True
    )
    back_rows = summed.reshape(senders, slot_count, -1)
    returned = lax.all_to_all(back_rows, "ep", split_axis=0, concat_axis=0, tiled=True)
    gathered = jnp.dot(
        selector, returned.reshape(experts * capacity, -1), preferred_element_type=jnp.float32
    )
    gathered = gathered.reshape(seq_count, choices_count, -1)
    routed = jnp.sum(route_weights[:, :, None] * gathered, axis=1)
    shared_g = jnp.dot(hidden, shared_gate, preferred_element_type=jnp.float32)
    shared_u = jnp.dot(hidden, shared_up, preferred_element_type=jnp.float32)
    shared_inner = (jax.nn.silu(shared_g) * shared_u).astype(jnp.bfloat16)
    shared_partial = jnp.dot(shared_inner, shared_down, preferred_element_type=jnp.float32)
    shared_result = lax.psum_scatter(
        shared_partial.astype(jnp.bfloat16), "tp", scatter_dimension=1, tiled=True
    ).astype(jnp.float32)
    own_hidden = lax.dynamic_slice_in_dim(hidden, core_index * half_width, half_width, 1)
    mixed_rows = RESIDUAL_SCALE * own_hidden.astype(jnp.float32) + routed + shared_result
    totals = lax.psum((jnp.sum(mixed_rows, axis=1), jnp.sum(mixed_rows * mixed_rows, axis=1)), "tp")
    row_mean = totals[0] / model_width
    row_var = totals[1] / model_width - row_mean * row_mean
    normed = (mixed_rows - row_mean[:, None]) * lax.rsqrt(row_var + NORM_EPS)[:, None]
    output = (normed * final_gain).astype(jnp.bfloat16)
    return (output, new_keys, new_values)


def solution(mesh):
    placed = (
        P("ep", None),
        P("ep", "tp", None, None),
        P("ep", "tp", None, None),
        P("ep"),
        P(None, "tp"),
        P(None, "tp"),
        P(None, "tp"),
        P("tp"),
        P("tp", None),
        P(),
        P(),
        P("ep", None),
        P("ep", None, "tp"),
        P("ep", None, "tp"),
        P("ep", "tp", None),
        P(None, "tp"),
        P(None, "tp"),
        P("tp", None),
        P("tp"),
    )
    return jax.shard_map(
        on_device,
        mesh=mesh,
        in_specs=placed,
        out_specs=(P("ep", "tp"), P("ep", "tp"), P("ep", "tp")),
        check_vma=False,
    )
```

profile of v0, /device:TPU:1, one launch (start us, length us, event | category | flops | bytes accessed | tf_op | source)
XLA Modules:
  0.0 174.3 jit_solution(5036537996058150898)
XLA Ops:
  7.2 0.0 copy-start
  7.2 0.0 copy-start.10
  7.2 0.0 all-reduce.3.cloned.1.call-start
  7.2 2.3 %convolution_convert_fusion.4 = bf16[64,512]{1,0:T(8,128)(2,1)S(1)} fusion(bf16[64,2048]{1,0:T(8,128)(2,1)} %param.19, bf16[2048,512]{1,0:T(8,128)(2,1)} %param.23), kind=kOutput, calls=%fused_computation.27 | convolution fusion | flops 134250496 | bytes 2424832 | tf_op jit(solution)/shard_map/dot_general | solution.py:71
  9.5 0.1 reshape.201
  9.7 0.0 copy-done.10
  9.7 0.1 iota_compare_fusion.3
  9.8 0.0 copy-start.11
  9.8 4.6 %fusion.2 = f32[64,8,1024]{2,1,0:T(8,128)S(1)} fusion(bf16[64,8,64]{2,1,0:T(8,128)(2,1)S(1)} %reshape.201, bf16[64,1,64,1024]{3,2,1,0:T(8,128)(2,1)} %param.20), kind=kOutput, calls=%fused_computation.2 | convolution fusion | flops 67108864 | bytes 10551296 | tf_op jit(solution)/shard_map/skgd,skdc->skgc/dot_general | solution.py:77
  14.4 0.0 copy-done.11
  14.4 3.0 %fusion.65 = (f32[64,8,8]{1,2,0:T(8,128)S(1)}, f32[64,8,8,128]{3,1,2,0:T(8,128)}) fusion(f32[8]{0:T(128)S(1)} %copy-done.11, f32[64,8,1024]{2,1,0:T(8,128)S(1)} %fusion.2, pred[64,1024]{1,0:T(8,128)(4,1)S(1)} %iota_compare_fusion.3), kind=kLoop, calls=%fused_computation.95 | loop fusion | flops 5763072 | bytes 4276256 | tf_op jit(solution)/shard_map/reduce_sum | solution.py:35
  17.4 0.0 copy-done.1
  17.4 0.1 copy.53
  17.5 0.2 fusion.58
  17.7 0.1 copy.54
  17.8 4.2 %fusion.14 = f32[64,8,8,128]{3,2,1,0:T(8,128)} fusion(f32[64,8,8,128]{3,1,2,0:T(8,128)} %get-tuple-element.11, f32[64,8,8]{2,1,0:T(8,128)S(1)} %copy.54), kind=kOutput, calls=%fused_computation.21 | convolution fusion | flops 805847040 | bytes 4210688 | tf_op jit(solution)/shard_map/...bi,ic->...bc/dot_general | solution.py:32
  22.0 2.7 %reshape.204 = f32[64,8,1024]{2,1,0:T(8,128)} reshape(f32[64,8,8,128]{3,2,1,0:T(8,128)} %fusion.14) | data formatting | bytes 4194304 | tf_op jit(solution)/shard_map/reshape | solution.py:39
  24.7 7.0 %fusion.19 = bf16[64,8,64]{2,1,0:T(8,128)(2,1)S(1)} fusion(bf16[64,1,64,1024]{3,2,1,0:T(8,128)(2,1)} %param.21, f32[64,8,1024]{2,1,0:T(8,128)} %reshape.204, f32[64,8,1024]{2,1,0:T(8,128)} %copy-done.1, f32[8]{0:T(128)S(1)} %copy-done.11, pred[64,1024]{1,0:T(8,128)(4,1)S(1)} %iota_compare_fusion.3), kind=kOutput, calls=%fused_computation.26 | convolution fusion | flops 73957376 | bytes 12714016 | tf_op jit(solution)/shard_map/skgc,skdc->skgd/dot_general | solution.py:87
  31.7 0.0 copy-start.8
  31.7 0.1 reshape.206
  31.9 0.0 copy-done
  31.9 1.2 convolution_convert_fusion.3
  33.1 0.0 all-reduce.3.cloned.1.call-update
  33.1 0.0 reduce-scatter.3.cloned.1.call-start
  33.1 0.0 copy-done.7
  33.2 0.1 copy.55
  33.3 0.1 eq.59
  33.4 0.2 fusion.23
  33.6 0.1 convert_element_type.118
  33.7 0.1 copy.56
  33.8 0.1 convert_reduce_fusion
  33.9 20.1 %all-reduce.3.cloned.1.call-done = bf16[64,2048]{1,0:T(8,128)(2,1)} async-done(((bf16[64,2048]{1,0:T(8,128)(2,1)}), bf16[64,2048]{1,0:T(8,128)(2,1)}) %all-reduce.3.cloned.1.call-update) | async-done | bytes 262160 | tf_op jit(solution)/shard_map/psum | solution.py:91
  54.0 0.0 copy-done.2
  54.0 1.1 fusion.42
  55.1 1.2 multiply_reduce_fusion
  56.3 0.0 copy-done.8
  56.3 1.1 multiply_convert_fusion
  57.4 0.7 convolution_convert_fusion.1
  58.1 0.0 copy-start.12
  58.1 53.6 %all_to_all.10 = bf16[16,32,2048]{2,1,0:T(8,128)(2,1)S(1)} all-to-all(bf16[16,32,2048]{2,1,0:T(8,128)(2,1)S(1)} %bitcast.62), channel_id=1, replica_groups=mesh['ep'=16,'tp'=2] {'ep'}, dimensions={0} | all-to-all | bytes 4194304 | tf_op jit(solution)/shard_map/all_to_all | solution.py:122
  111.7 1.3 copy-done.3
  113.0 0.0 copy-done.12
  113.0 0.7 fusion.31
  113.7 5.8 %convolution_convert_fusion = bf16[512,2048]{1,0:T(8,128)(2,1)} fusion(bf16[512,2048]{1,0:T(8,128)(2,1)} %bitcast.64, bf16[1,256,2048]{2,1,0:T(8,128)(2,1)} %param.33, bf16[1,2048,256]{2,1,0:T(8,128)(2,1)} %param.32, f32[512,256]{1,0:T(8,128)S(1)} %fusion.31), kind=kOutput, calls=%fused_computation.6 | convolution fusion | flops 1075576832 | bytes 6815744 | tf_op jit(solution)/shard_map/dot_general | solution.py:128
  119.6 0.0 reduce-scatter.3.cloned.1.call-update
  119.6 10.6 %reduce-scatter.3.cloned.1.call-done = bf16[512,1024]{1,0:T(8,128)(2,1)} async-done(((bf16[512,2048]{1,0:T(8,128)(2,1)}), bf16[512,1024]{1,0:T(8,128)(2,1)}) %reduce-scatter.3.cloned.1.call-update) | async-done | bytes 1048592 | tf_op jit(solution)/shard_map/reduce_scatter | solution.py:129
  130.2 6.5 %all-to-all-start.1 = ((bf16[16,32,1024]{2,1,0:T(8,128)(2,1)}), bf16[16,32,1024]{2,1,0:T(8,128)(2,1)}, u32[]{:S(2)}, u32[]{:S(2)}) async-start(bf16[16,32,1024]{2,1,0:T(8,128)(2,1)} %bitcast.65), calls=%async_computation.2 | async-start | bytes 2097152 | tf_op jit(solution)/shard_map/all_to_all | solution.py:133
  136.7 0.0 reduce-scatter.5.cloned.1.call-start
  136.7 0.0 copy-done.4
  136.7 0.8 convolution_convert_fusion.5
  137.6 0.0 copy-done.5
  137.6 0.8 convolution_convert_fusion.6
  138.4 1.5 fusion.67
  139.9 3.1 %convolution_convert_fusion.2 = bf16[64,2048]{1,0:T(8,128)(2,1)} fusion(bf16[256,2048]{1,0:T(8,128)(2,1)} %param.36, bf16[64,2048]{1,0:T(8,128)(2,1)S(1)} %multiply_convert_fusion, bf16[2048,256]{1,0:T(8,128)(2,1)} %param.35, f32[64,256]{1,0:T(8,128)S(1)} %fusion.67), kind=kOutput, calls=%fused_computation.8 | convolution fusion | flops 134447104 | bytes 2686976 | tf_op jit(solution)/shard_map/dot_general | solution.py:142
  143.0 0.0 reduce-scatter.5.cloned.1.call-update
  143.0 0.0 copy-done.6
  143.1 0.2 fusion.26
  143.3 15.1 %all-to-all-done.1 = bf16[16,32,1024]{2,1,0:T(8,128)(2,1)} async-done(((bf16[16,32,1024]{2,1,0:T(8,128)(2,1)}), bf16[16,32,1024]{2,1,0:T(8,128)(2,1)}, u32[]{:S(2)}, u32[]{:S(2)}) %all-to-all-start.1) | async-done | bytes 1048608 | tf_op jit(solution)/shard_map/all_to_all | solution.py:133
  158.4 1.7 fusion.17
  160.1 0.0 reduce-scatter.5.cloned.1.call-done
  160.1 1.1 fusion.64
  161.2 5.7 %all-reduce = (f32[64]{0:T(128)S(1)}, f32[64]{0:T(128)S(1)}) all-reduce(f32[64]{0:T(128)S(1)} %get-tuple-element.4, f32[64]{0:T(128)S(1)} %get-tuple-element.3), channel_id=1, replica_groups=mesh['ep'=16,'tp'=2] {'tp'}, use_global_device_ids=true, to_apply=%region_14.15 | all-reduce | flops 128 | bytes 1024 | tf_op jit(solution)/shard_map/psum | solution.py:148
  167.0 0.0 copy-done.9
  167.0 0.8 multiply_convert_fusion.1
  (15 shorter events, 0.1 us)
Async XLA Ops:
  7.2 24.7 %copy-start = (bf16[512,2048]{1,0:T(8,128)(2,1)S(1)}, bf16[512,2048]{1,0:T(8,128)(2,1)}, u32[]{:S(2)}) copy-start(bf16[512,2048]{1,0:T(8,128)(2,1)} %param.27) | copy-start | bytes 6291460
  7.2 2.5 %copy-start.10 = (s32[64]{0:T(128)S(1)}, s32[64]{0:T(128)}, u32[]{:S(2)}) copy-start(s32[64]{0:T(128)} %param.22) | copy-start | bytes 772
  7.2 46.8 %all-reduce.3.cloned.1.call-start = ((), (), s32[]{:S(2)}) async-start(), calls=%async_computation.4 | async-start | bytes 524288 | tf_op jit(solution)/shard_map/psum | solution.py:91
  9.8 4.6 %copy-start.11 = (f32[8]{0:T(128)S(1)}, f32[8]{0:T(128)}, u32[]{:S(2)}) copy-start(f32[8]{0:T(128)} %param.26) | copy-start | bytes 100
  14.4 3.0 %copy-start.1 = (f32[64,8,1024]{2,1,0:T(8,128)}, f32[64,8,1024]{2,1,0:T(8,128)S(1)}, u32[]{:S(2)}) copy-start(f32[64,8,1024]{2,1,0:T(8,128)S(1)} %fusion.2) | copy-start | bytes 6291460
  31.7 1.4 copy-start.7
  31.7 22.2 %copy-start.2 = (bf16[64,2048]{1,0:T(8,128)(2,1)S(1)}, bf16[64,2048]{1,0:T(8,128)(2,1)}, u32[]{:S(2)}) copy-start(bf16[64,2048]{1,0:T(8,128)(2,1)} %param.19) | copy-start | bytes 786436
  31.7 24.6 %copy-start.8 = (f32[2048]{0:T(1024)S(1)}, f32[2048]{0:T(1024)}, u32[]{:S(2)}) copy-start(f32[2048]{0:T(1024)} %param.28) | copy-start | bytes 24580
  33.1 97.1 %reduce-scatter.3.cloned.1.call-start = ((), (), s32[]{:S(2)}) async-start(), calls=%async_computation.5 | async-start | bytes 3145728 | tf_op jit(solution)/shard_map/reduce_scatter | solution.py:129
  58.1 54.9 %copy-start.12 = (bf16[1,2048,256]{2,1,0:T(8,128)(2,1)S(1)}, bf16[1,2048,256]{2,1,0:T(8,128)(2,1)}, u32[]{:S(2)}) copy-start(bf16[1,2048,256]{2,1,0:T(8,128)(2,1)} %param.31) | copy-start | bytes 3145732
  111.7 1.3 copy-start.3
  119.6 17.2 %copy-start.4 = (bf16[2048,64]{0,1:T(8,128)(2,1)S(1)}, bf16[2048,64]{0,1:T(8,128)(2,1)}, u32[]{:S(2)}) copy-start(bf16[2048,64]{0,1:T(8,128)(2,1)} %param.25) | copy-start | bytes 786436
  119.6 18.0 %copy-start.5 = (bf16[2048,64]{0,1:T(8,128)(2,1)S(1)}, bf16[2048,64]{0,1:T(8,128)(2,1)}, u32[]{:S(2)}) copy-start(bf16[2048,64]{0,1:T(8,128)(2,1)} %param.24) | copy-start | bytes 786436
  130.2 28.2 %all-to-all-start.1 = ((bf16[16,32,1024]{2,1,0:T(8,128)(2,1)}), bf16[16,32,1024]{2,1,0:T(8,128)(2,1)}, u32[]{:S(2)}, u32[]{:S(2)}) async-start(bf16[16,32,1024]{2,1,0:T(8,128)(2,1)} %bitcast.65), calls=%async_computation.2 | async-start | bytes 2097152 | tf_op jit(solution)/shard_map/all_to_all | solution.py:133
  136.7 23.4 %reduce-scatter.5.cloned.1.call-start = ((), (), s32[]{:S(2)}) async-start(), calls=%async_computation.6 | async-start | bytes 393216 | tf_op jit(solution)/shard_map/reduce_scatter | solution.py:143
  138.4 4.6 %copy-start.6 = (bf16[2048,16]{0,1:T(8,128)(2,1)S(1)}, bf16[2048,16]{0,1:T(8,128)(2,1)}, u32[]{:S(2)}) copy-start(bf16[2048,16]{0,1:T(8,128)(2,1)} %param.29) | copy-start | bytes 196612
  143.0 24.0 %copy-start.9 = (f32[1024]{0:T(1024)S(1)}, f32[1024]{0:T(1024)}, u32[]{:S(2)}) copy-start(f32[1024]{0:T(1024)} %param.37) | copy-start | bytes 12292
Sparse Core Ops, SparseCore 0:
  33.2 20.6 all-reduce.2
  119.7 10.4 reduce-scatter.2
  143.2 9.2 reduce-scatter.4
where the time goes:
time: 176 us; the launch traced here: 174 us
  blocking collectives  59.3 us (34%)
  waiting for transfers between devices  45.8 us (26%)
  matrix products  35 us (20%)
  between operations  14 us (8%)
  other arithmetic  8.58 us (5%)
  starting transfers between devices  6.62 us (4%)
  local copies, waits for them, and re-layouts  4.99 us (3%)
    all_to_all x1, blocking collectives, on_device(): lax.all_to_all(outgoing, 'ep', split_axis=0, concat_axis=0, tiled=True)  53.6 us
    psum x1, waiting for transfers between devices, on_device(): lax.psum(jnp.dot(attended, out_weight, preferred_element_type=jnp.float32...  20.1 us
    all_to_all x1, waiting for transfers between devices, on_device(): lax.all_to_all(back_rows, 'ep', split_axis=0, concat_axis=0, tiled=True)  15.1 us
    reduce_scatter x1, waiting for transfers between devices, on_device(): lax.psum_scatter(partial_value.astype(jnp.bfloat16), 'tp', scatter_dimens...  10.6 us
    dot_general x1, matrix products, on_device(): jnp.einsum('skgc,skdc->skgd', stick_weight, cache_values, preferred_eleme...  7 us
    all_to_all x1, starting transfers between devices, on_device(): lax.all_to_all(back_rows, 'ep', split_axis=0, concat_axis=0, tiled=True)  6.5 us
    dot_general x1, matrix products, on_device(): jnp.dot(inner, expert_down[0], preferred_element_type=jnp.float32)  5.83 us
    psum x1, blocking collectives, on_device(): lax.psum((jnp.sum(mixed_rows, axis=1), jnp.sum(mixed_rows * mixed_rows, a...  5.74 us
  transfers between devices with their start and end apart: 4, of which 3 were waited for; matrix products, arithmetic and copies ran while one was open for 5% of the time, Pallas kernels for 0%

commit v1 on v0

v1 whole, which is shorter than its diff:
```python
import functools
import math

import jax
import jax.numpy as jnp
from jax import lax
from jax.experimental import pallas as pl
from jax.experimental.pallas import tpu as pltpu
from jax.sharding import PartitionSpec as P

RESIDUAL_SCALE = 2.0**0.25
ROUTE_SCALE = 2.5
NORM_EPS = 1e-05


def layer_norm(values, gain_vec):
    row_mean = jnp.mean(values, axis=-1, keepdims=True)
    centered = values - row_mean
    row_var = jnp.mean(centered * centered, axis=-1, keepdims=True)
    return centered * lax.rsqrt(row_var + NORM_EPS) * gain_vec


def strictly_later(size):
    row_pos = lax.broadcasted_iota(jnp.int32, (size, size), 0)
    col_pos = lax.broadcasted_iota(jnp.int32, (size, size), 1)
    return (row_pos > col_pos).astype(jnp.float32)


def later_totals(log_keep):
    lead = log_keep.shape[:-1]
    length = log_keep.shape[-1]
    block_size = math.gcd(length, 128)
    block_count = length // block_size
    blocked = log_keep.reshape(lead + (block_count, block_size))
    inside = jnp.einsum(
        "...bi,ic->...bc", blocked, strictly_later(block_size), precision=lax.Precision.HIGHEST
    )
    block_total = jnp.sum(blocked, axis=-1)
    after = jnp.einsum(
        "...i,ic->...c", block_total, strictly_later(block_count), precision=lax.Precision.HIGHEST
    )
    return (inside + after[..., None]).reshape(lead + (length,))


LANES = 128
VMEM_BYTES = 67043328
BF16 = jnp.bfloat16
F32 = jnp.float32


def grid_of(count):
    side = round(count ** (1.0 / 3.0))
    if side**3 == count:
        return side, side, side
    if count % 4 == 0:
        return count // 4, 2, 2
    return count, 1, 1


def moe_kernel(
    dims,
    part_ref,
    inputs_ref,
    mask_ref,
    attend_gain_ref,
    final_gain_ref,
    router_hbm,
    gate_hbm,
    up_hbm,
    down_hbm,
    sgate_hbm,
    sup_hbm,
    sdown_hbm,
    out_ref,
    part_in,
    rows_all,
    router_w,
    gate_w,
    up_w,
    down_w,
    sgate_w,
    sup_w,
    sdown_w,
    own_sum,
    pair_out,
    pair_in,
    shared_mine,
    first_a,
    first_b,
    second_a,
    second_b,
    third,
    stats_out,
    stats_in,
    load_sem,
    send_sem,
    part_sem,
    full_sem,
    a_sem,
    b_sem,
    pf_sem,
    pa_sem,
    pb_sem,
    pair_sem,
    fa_sem,
    fb_sem,
    sa_sem,
    sb_sem,
    third_sem,
    stats_sem,
):
    nz, ny, nx = dims
    rows, width = inputs_ref.shape
    half = rows // 2
    dh = width // 2
    dq = dh // 2
    plane = ny * nx * rows
    core = lax.axis_index("tp")
    other = 1 - core
    me = lax.axis_index("ep")
    x = me % nx
    y = (me // nx) % ny
    z = me // (nx * ny)

    def index(dz, dy, dx):
        return (((z + nz - dz) % nz) * ny + (y + ny - dy) % ny) * nx + (x + nx - dx) % nx

    def rel(dz, dy, dx):
        return (dz * ny + dy) * nx + dx

    def to_z(step):
        return {"ep": (((z + step) % nz) * ny + y) * nx + x}

    def to_y(step):
        return {"ep": (z * ny + (y + step) % ny) * nx + x}

    def to_x(step):
        return {"ep": (z * ny + y) * nx + (x + step) % nx}

    partner = {"tp": other}
    loads = []
    for i, (src, dst) in enumerate(
        (
            (router_hbm, router_w),
            (sgate_hbm, sgate_w),
            (sup_hbm, sup_w),
            (sdown_hbm, sdown_w),
            (gate_hbm, gate_w),
            (up_hbm, up_w),
            (down_hbm, down_w),
        )
    ):
        copy = pltpu.make_async_copy(src, dst, load_sem.at[i])
        copy.start()
        loads.append(copy)

    barrier = pltpu.get_barrier_semaphore()
    greeted = [partner]
    greeted += [to_z(i) for i in range(1, nz)]
    greeted += [to_y(i) for i in range(1, ny)]
    greeted += [to_x(i) for i in range(1, nx)]
    for device in greeted:
        pl.semaphore_signal(barrier, inc=1, device_id=device, device_id_type=pl.DeviceIdType.MESH)
    pl.semaphore_wait(barrier, len(greeted))

    sent = []

    def remote(src, dst, recv, device):
        copy = pltpu.make_async_remote_copy(
            src_ref=src,
            dst_ref=dst,
            send_sem=send_sem.at[len(sent)],
            recv_sem=recv,
            device_id=device,
            device_id_type=pl.DeviceIdType.MESH,
        )
        copy.start()
        sent.append(copy)

    def arrived(dst, recv):
        pltpu.make_async_remote_copy(
            src_ref=dst,
            dst_ref=dst,
            send_sem=send_sem.at[0],
            recv_sem=recv,
            device_id=partner,
            device_id_type=pl.DeviceIdType.MESH,
        ).wait_recv()

    def mult(value, by):
        return pl.multiple_of(value, by)

    remote(part_ref.at[pl.ds(mult(other * half, half), half)], part_in, part_sem.at[0], partner)
    arrived(part_in, part_sem.at[0])
    own_half = pl.ds(mult(core * half, half), half)
    attention = part_ref[own_half, :].astype(F32) + part_in[...].astype(F32)
    hidden = layer_norm(
        RESIDUAL_SCALE * inputs_ref[own_half, :].astype(F32) + attention, attend_gain_ref[...]
    ).astype(BF16)
    loads[0].wait()
    probs = jax.nn.sigmoid(jnp.dot(hidden, router_w[...], preferred_element_type=F32))
    chosen = probs * mask_ref[own_half, :]
    weights = ROUTE_SCALE * chosen / jnp.sum(chosen, axis=1, keepdims=True)
    mine = pl.ds(mult(me * rows + core * half, half), half)
    rows_all[mine, pl.ds(0, width)] = hidden
    rows_all[mine, pl.ds(width, LANES)] = weights.astype(BF16)

    full_cols = pl.ds(0, width + LANES)
    a_cols = pl.ds(0, dh)
    b_cols = pl.ds(dh, dh + LANES)

    def slot(dz, dy, dx, cols, who=core):
        return rows_all.at[pl.ds(mult(index(dz, dy, dx) * rows + who * half, half), half), cols]

    def spread(dz, dy, dx, cols, targets, sems):
        block = slot(dz, dy, dx, cols)
        for device, sem_index in targets:
            remote(block, block, sems.at[sem_index], device)

    def have_full(dz):
        spread(dz, 0, 0, a_cols, [(to_y(i), rel(dz, i, 0)) for i in range(1, ny)], a_sem)
        spread(dz, 0, 0, b_cols, [(to_x(i), rel(dz, 0, i)) for i in range(1, nx)], b_sem)
        spread(dz, 0, 0, a_cols, [(to_x(i), rel(dz, 0, i)) for i in range(1, nx)], a_sem)
        spread(dz, 0, 0, b_cols, [(to_y(i), rel(dz, i, 0)) for i in range(1, ny)], b_sem)
        spread(dz, 0, 0, full_cols, [(partner, rel(dz, 0, 0))], pf_sem)

    def have_middle(dz):
        for dy in range(1, ny):
            arrived(slot(dz, dy, 0, a_cols), a_sem.at[rel(dz, dy, 0)])
            spread(dz, dy, 0, a_cols, [(to_x(i), rel(dz, dy, i)) for i in range(1, nx)], a_sem)
            spread(dz, dy, 0, a_cols, [(partner, rel(dz, dy, 0))], pa_sem)
        for dx in range(1, nx):
            arrived(slot(dz, 0, dx, b_cols), b_sem.at[rel(dz, 0, dx)])
            spread(dz, 0, dx, b_cols, [(to_y(i), rel(dz, i, dx)) for i in range(1, ny)], b_sem)
            spread(dz, 0, dx, b_cols, [(partner, rel(dz, 0, dx))], pb_sem)

    def have_last(dz):
        for dy in range(ny):
            for dx in range(nx):
                if dx > 0:
                    arrived(slot(dz, dy, dx, a_cols), a_sem.at[rel(dz, dy, dx)])
                    spread(dz, dy, dx, a_cols, [(partner, rel(dz, dy, dx))], pa_sem)
                if dy > 0:
                    arrived(slot(dz, dy, dx, b_cols), b_sem.at[rel(dz, dy, dx)])
                    spread(dz, dy, dx, b_cols, [(partner, rel(dz, dy, dx))], pb_sem)
        for dy in range(ny):
            for dx in range(nx):
                if dy + dx == 0:
                    if dz > 0:
                        arrived(slot(dz, 0, 0, full_cols, other), pf_sem.at[rel(dz, 0, 0)])
                    continue
                arrived(slot(dz, dy, dx, a_cols, other), pa_sem.at[rel(dz, dy, dx)])
                arrived(slot(dz, dy, dx, b_cols, other), pb_sem.at[rel(dz, dy, dx)])

    spread(0, 0, 0, full_cols, [(to_z(i), rel(i, 0, 0)) for i in range(1, nz)], full_sem)
    have_full(0)
    for dz in range(1, nz):
        arrived(slot(dz, 0, 0, full_cols), full_sem.at[rel(dz, 0, 0)])
        have_full(dz)
        have_middle(dz - 1)
    arrived(slot(0, 0, 0, full_cols, other), pf_sem.at[rel(0, 0, 0)])

    keep_cols = pl.ds(mult(core * dh, dh), dh)
    give_cols = pl.ds(mult(other * dh, dh), dh)
    own_rows = pl.ds(mult(me * rows, rows), rows)
    for copy in loads[1:]:
        copy.wait()
    own_hidden = rows_all[own_rows, pl.ds(0, width)]
    shared_g = jnp.dot(own_hidden, sgate_w[...], preferred_element_type=F32)
    shared_u = jnp.dot(own_hidden, sup_w[...], preferred_element_type=F32)
    shared_inner = (jax.nn.silu(shared_g) * shared_u).astype(BF16)
    shared_mine[...] = jnp.dot(shared_inner, sdown_w[:, keep_cols], preferred_element_type=F32)
    shared_give = jnp.dot(shared_inner, sdown_w[:, give_cols], preferred_element_type=F32)
    have_middle(nz - 1)

    chunk = math.gcd(plane, 256)

    def plane_start(dz):
        return ((z + nz - dz) % nz) * plane

    def compute(dz):
        start = plane_start(dz)

        def one(i, carry):
            part = pl.ds(mult(start + i * chunk, chunk), chunk)
            tokens = rows_all[part, pl.ds(0, width)]
            gate_act = jnp.dot(tokens, gate_w[...], preferred_element_type=F32)
            up_act = jnp.dot(tokens, up_w[...], preferred_element_type=F32)
            inner = (jax.nn.silu(gate_act) * up_act).astype(BF16)
            table = rows_all[part, pl.ds(width, LANES)].astype(F32)
            lane = lax.broadcasted_iota(jnp.int32, (chunk, LANES), 1)
            scale = jnp.sum(jnp.where(lane == me, table, 0.0), axis=1, keepdims=True)
            pair_out[part, :] = (
                scale * jnp.dot(inner, down_w[:, give_cols], preferred_element_type=F32)
            ).astype(BF16)
            own_sum[part, :] = (
                scale * jnp.dot(inner, down_w[:, keep_cols], preferred_element_type=F32)
            ).astype(BF16)
            return carry

        lax.fori_loop(0, plane // chunk, one, 0)
        if dz == 0:
            pair_out[own_rows, :] = (pair_out[own_rows, :].astype(F32) + shared_give).astype(BF16)
        whole = pl.ds(mult(start, plane), plane)
        remote(pair_out.at[whole], pair_in.at[whole], pair_sem.at[dz], partner)

    a_part = pl.ds(0, dq)
    b_part = pl.ds(dq, dq)

    def block(dz, dy, dx):
        return pl.ds(mult(index(dz, dy, dx) * rows, rows), rows)

    def first(dz):
        whole = pl.ds(mult(plane_start(dz), plane), plane)
        arrived(pair_in.at[whole], pair_sem.at[dz])

        def one(i, carry):
            part = pl.ds(mult(plane_start(dz) + i * rows, rows), rows)
            own_sum[part, :] = (
                own_sum[part, :].astype(F32) + pair_in[part, :].astype(F32)
            ).astype(BF16)
            return carry

        lax.fori_loop(0, plane // rows, one, 0)
        for step in range(1, nx):
            for dy in range(ny - 1, -1, -1):
                at = (dz * (nx - 1) + step - 1) * ny + dy
                remote(
                    own_sum.at[block(dz, dy, nx - step), a_part],
                    first_a.at[at],
                    fa_sem.at[at],
                    to_x(step),
                )
        for step in range(1, ny):
            for dx in range(nx - 1, -1, -1):
                at = (dz * (ny - 1) + step - 1) * nx + dx
                remote(
                    own_sum.at[block(dz, ny - step, dx), b_part],
                    first_b.at[at],
                    fb_sem.at[at],
                    to_y(step),
                )

    def add_in(where, cols, buffer, sems, places):
        total = own_sum[where, cols].astype(F32)
        for at in places:
            arrived(buffer.at[at], sems.at[at])
            total = total + buffer[at].astype(F32)
        own_sum[where, cols] = total.astype(BF16)

    def second(dz):
        for dy in range(ny - 1, -1, -1):
            places = [(dz * (nx - 1) + step - 1) * ny + dy for step in range(1, nx)]
            add_in(block(dz, dy, 0), a_part, first_a, fa_sem, places)
            if dy > 0:
                at = dz * (ny - 1) + ny - dy - 1
                remote(
                    own_sum.at[block(dz, dy, 0), a_part],
                    second_a.at[at],
                    sa_sem.at[at],
                    to_y(ny - dy),
                )
        for dx in range(nx - 1, -1, -1):
            places = [(dz * (ny - 1) + step - 1) * nx + dx for step in range(1, ny)]
            add_in(block(dz, 0, dx), b_part, first_b, fb_sem, places)
            if dx > 0:
                at = dz * (nx - 1) + nx - dx - 1
                remote(
                    own_sum.at[block(dz, 0, dx), b_part],
                    second_b.at[at],
                    sb_sem.at[at],
                    to_x(nx - dx),
                )

    def last(dz):
        places = [dz * (ny - 1) + step - 1 for step in range(1, ny)]
        add_in(block(dz, 0, 0), a_part, second_a, sa_sem, places)
        places = [dz * (nx - 1) + step - 1 for step in range(1, nx)]
        add_in(block(dz, 0, 0), b_part, second_b, sb_sem, places)
        if dz > 0:
            remote(
                own_sum.at[block(dz, 0, 0)], third.at[dz - 1], third_sem.at[dz - 1], to_z(nz - dz)
            )

    order = list(range(nz))
    for k in range(nz + 3):
        if k < nz:
            have_last(order[k])
            compute(order[k])
        if 1 <= k < nz + 1:
            first(order[k - 1])
        if 2 <= k < nz + 2:
            second(order[k - 2])
        if 3 <= k:
            last(order[k - 3])

    total = own_sum[own_rows, :].astype(F32) + shared_mine[...]
    total = total + RESIDUAL_SCALE * rows_all[own_rows, keep_cols].astype(F32)
    for i in range(nz - 1):
        arrived(third.at[i], third_sem.at[i])
        total = total + third[i].astype(F32)
    lane = lax.broadcasted_iota(jnp.int32, (rows, LANES), 1)
    sum_one = jnp.sum(total, axis=1, keepdims=True)
    sum_two = jnp.sum(total * total, axis=1, keepdims=True)
    stats_out[...] = jnp.where(lane == 0, sum_one, sum_two)
    remote(stats_out, stats_in, stats_sem.at[0], partner)
    arrived(stats_in, stats_sem.at[0])
    row_mean = (sum_one + stats_in[:, 0:1]) / width
    row_var = (sum_two + stats_in[:, 1:2]) / width - row_mean * row_mean
    normed = (total - row_mean) * lax.rsqrt(row_var + NORM_EPS)
    out_ref[...] = (normed * final_gain_ref[...]).astype(BF16)
    for copy in sent:
        copy.wait_send()


def moe_layer(
    count, part, inputs, mask, attend_gain, final_gain, router, gate, up, down, sgate, sup, sdown
):
    dims = grid_of(count)
    nz, ny, nx = dims
    rows, width = inputs.shape
    half = rows // 2
    dh = width // 2
    dq = dh // 2
    everyone = count * rows
    sends = 3 + (nz - 1) + 2 * (count + nz) + nz * (nx - 1 + ny - 1) * 2 + 2 * count
    sends += 2 * nz * ny * nx + nz + 2 * nz * (ny + nx + ny * nx) + nz
    vmem = pl.BlockSpec(memory_space=pltpu.VMEM)
    anywhere = pl.BlockSpec(memory_space=pl.ANY)
    n1a, n1b = max(1, nz * (nx - 1) * ny), max(1, nz * (ny - 1) * nx)
    n2a, n2b = max(1, nz * (ny - 1)), max(1, nz * (nx - 1))
    n3 = max(1, nz - 1)
    dma = pltpu.SemaphoreType.DMA
    return pl.pallas_call(
        functools.partial(moe_kernel, dims),
        out_shape=jax.ShapeDtypeStruct((rows, dh), BF16),
        in_specs=[vmem] * 5 + [anywhere] * 7,
        out_specs=vmem,
        scratch_shapes=[
            pltpu.VMEM((half, width), BF16),
            pltpu.VMEM((everyone, width + LANES), BF16),
            pltpu.VMEM(router.shape, BF16),
            pltpu.VMEM(gate.shape, BF16),
            pltpu.VMEM(up.shape, BF16),
            pltpu.VMEM(down.shape, BF16),
            pltpu.VMEM(sgate.shape, BF16),
            pltpu.VMEM(sup.shape, BF16),
            pltpu.VMEM(sdown.shape, BF16),
            pltpu.VMEM((everyone, dh), BF16),
            pltpu.VMEM((everyone, dh), BF16),
            pltpu.VMEM((everyone, dh), BF16),
            pltpu.VMEM((rows, dh), F32),
            pltpu.VMEM((n1a, rows, dq), BF16),
            pltpu.VMEM((n1b, rows, dq), BF16),
            pltpu.VMEM((n2a, rows, dq), BF16),
            pltpu.VMEM((n2b, rows, dq), BF16),
            pltpu.VMEM((n3, rows, dh), BF16),
            pltpu.VMEM((rows, LANES), F32),
            pltpu.VMEM((rows, LANES), F32),
            dma((7,)),
            dma((sends,)),
            dma((1,)),
            dma((count,)),
            dma((count,)),
            dma((count,)),
            dma((count,)),
            dma((count,)),
            dma((count,)),
            dma((nz,)),
            dma((n1a,)),
            dma((n1b,)),
            dma((n2a,)),
            dma((n2b,)),
            dma((n3,)),
            dma((1,)),
        ],
        compiler_params=pltpu.CompilerParams(
            collective_id=0, has_side_effects=True, vmem_limit_bytes=VMEM_BYTES
        ),
    )(part, inputs, mask, attend_gain, final_gain, router, gate, up, down, sgate, sup, sdown)


def on_device(
    inputs,
    cache_keys,
    cache_values,
    lengths,
    query_weight,
    key_weight,
    value_weight,
    head_bias,
    out_weight,
    attend_gain,
    router_weight,
    routes,
    expert_gate,
    expert_up,
    expert_down,
    shared_gate,
    shared_up,
    shared_down,
    final_gain,
):
    seq_count, model_width = inputs.shape
    key_heads, head_size, cache_length = cache_keys.shape[1:]
    query_heads = head_bias.shape[0]
    groups = query_heads // key_heads
    experts = router_weight.shape[1]
    query = jnp.dot(inputs, query_weight, preferred_element_type=jnp.float32).astype(jnp.bfloat16)
    query = query.reshape(seq_count, key_heads, groups, head_size)
    new_keys = jnp.dot(inputs, key_weight, preferred_element_type=jnp.float32).astype(jnp.bfloat16)
    new_values = jnp.dot(inputs, value_weight, preferred_element_type=jnp.float32).astype(
        jnp.bfloat16
    )
    scores = jnp.einsum("skgd,skdc->skgc", query, cache_keys, preferred_element_type=jnp.float32)
    scores = scores * head_size ** (-0.5) + head_bias.reshape(key_heads, groups)[None, :, :, None]
    usable = (
        lax.broadcasted_iota(jnp.int32, (1, 1, 1, cache_length), 3) < lengths[:, None, None, None]
    )
    log_keep = jnp.where(usable, jax.nn.log_sigmoid(-scores), 0.0)
    later_sum = later_totals(log_keep)
    stick_weight = jnp.where(usable, jnp.exp(jax.nn.log_sigmoid(scores) + later_sum), 0.0).astype(
        jnp.bfloat16
    )
    attended = jnp.einsum(
        "skgc,skdc->skgd", stick_weight, cache_values, preferred_element_type=jnp.float32
    )
    attended = attended.astype(jnp.bfloat16).reshape(seq_count, query_heads * head_size)
    part = jnp.dot(attended, out_weight, preferred_element_type=jnp.float32).astype(jnp.bfloat16)
    lanes = lax.broadcasted_iota(jnp.int32, (1, 1, LANES), 2)
    mask = jnp.sum((routes[:, :, None] == lanes).astype(jnp.float32), axis=1)
    router = jnp.pad(router_weight, ((0, 0), (0, LANES - experts)))
    output = moe_layer(
        lax.axis_size("ep"),
        part,
        inputs,
        mask,
        attend_gain[None, :],
        final_gain[None, :],
        router,
        expert_gate[0],
        expert_up[0],
        expert_down[0],
        shared_gate,
        shared_up,
        shared_down,
    )
    return (output, new_keys, new_values)


def solution(mesh):
    placed = (
        P("ep", None),
        P("ep", "tp", None, None),
        P("ep", "tp", None, None),
        P("ep"),
        P(None, "tp"),
        P(None, "tp"),
        P(None, "tp"),
        P("tp"),
        P("tp", None),
        P(),
        P(),
        P("ep", None),
        P("ep", None, "tp"),
        P("ep", None, "tp"),
        P("ep", "tp", None),
        P(None, "tp"),
        P(None, "tp"),
        P("tp", None),
        P("tp"),
    )
    return jax.shard_map(
        on_device,
        mesh=mesh,
        in_specs=placed,
        out_specs=(P("ep", "tp"), P("ep", "tp"), P("ep", "tp")),
        check_vma=False,
    )
```

time: 176 us -> 102 us (0.58)
  Pallas kernels: 0 us -> 66.8 us
  blocking collectives: 59.3 us -> 0 us
  waiting for transfers between devices: 45.8 us -> 0 us
  between operations: 14 us -> 0.72 us
  matrix products: 35 us -> 24 us
  starting transfers between devices: 6.62 us -> 0 us
  other arithmetic: 8.58 us -> 3.79 us
    pallas_call x0 -> x1, Pallas kernels: none -> 66.8 us  [moe_layer(): pl.pallas_call(functools.partial(moe_kernel, dims), out_shape=jax.ShapeDt...]
    all_to_all x1 -> x0, blocking collectives: 53.6 us -> none  [on_device(): lax.all_to_all(outgoing, 'ep', split_axis=0, concat_axis=0, tiled=True)]
    psum x1 -> x0, waiting for transfers between devices: 20.1 us -> none  [on_device(): lax.psum(jnp.dot(attended, out_weight, preferred_element_type=jnp.float32...]
    all_to_all x1 -> x0, waiting for transfers between devices: 15.1 us -> none  [on_device(): lax.all_to_all(back_rows, 'ep', split_axis=0, concat_axis=0, tiled=True)]
    dot_general x8 -> x0, matrix products: 14 us -> none  [the longest x1 5.83 us: on_device(): jnp.dot(inner, expert_down[0], preferred_element_type=jnp.float32)]
    reduce_scatter x2 -> x0, waiting for transfers between devices: 10.6 us -> none  [the longest x1 10.6 us: on_device(): lax.psum_scatter(partial_value.astype(jnp.bfloat16), 'tp', scatter_dimens...]
    all_to_all x1 -> x0, starting transfers between devices: 6.5 us -> none  [on_device(): lax.all_to_all(back_rows, 'ep', split_axis=0, concat_axis=0, tiled=True)]
    psum x1 -> x0, blocking collectives: 5.74 us -> none  [on_device(): lax.psum((jnp.sum(mixed_rows, axis=1), jnp.sum(mixed_rows * mixed_rows, a...]
  transfers between devices with their start and end apart: 4 -> 0, of which waited for: 3 -> 0; matrix products, arithmetic and copies ran while one was open for 5% -> 0% of each run, Pallas kernels for 0% -> 0%
where the time goes in v1:
time: 102 us; the launch traced here: 101 us
  Pallas kernels  66.8 us (65%)
  matrix products  24 us (24%)
  local copies, waits for them, and re-layouts  5.99 us (6%)
  other arithmetic  3.79 us (4%)
    pallas_call x1, Pallas kernels, moe_layer(): pl.pallas_call(functools.partial(moe_kernel, dims), out_shape=jax.ShapeDt...  66.8 us
    dot_general x1, matrix products, on_device(): jnp.einsum('skgc,skdc->skgd', stick_weight, cache_values, preferred_eleme...  6.37 us
    dot_general x1, matrix products, on_device(): jnp.einsum('skgd,skdc->skgc', query, cache_keys, preferred_element_type=j...  4.58 us
    dot_general x1, matrix products, later_totals(): jnp.einsum('...bi,ic->...bc', blocked, strictly_later(block_size), precis...  4.22 us
    reduce_sum x1, other arithmetic, later_totals(): block_total = jnp.sum(blocked, axis=-1)  2.96 us
    dot_general x1, matrix products, on_device(): jnp.dot(attended, out_weight, preferred_element_type=jnp.float32)  2.78 us
    reshape x1, local copies, waits for them, and re-layouts, later_totals(): return (inside + after[..., None]).reshape(lead + (length,))  2.68 us
    dot_general x1, matrix products, on_device(): jnp.dot(inputs, query_weight, preferred_element_type=jnp.float32)  2.16 us

profile of v1, /device:TPU:1, one launch (start us, length us, event | category | flops | bytes accessed | tf_op | source)
XLA Modules:
  0.0 101.3 jit_solution(306769772472748515)
XLA Ops:
  0.6 2.2 %convolution_convert_fusion.1 = bf16[64,512]{1,0:T(8,128)(2,1)S(1)} fusion(bf16[64,2048]{1,0:T(8,128)(2,1)} %inputs_ref.1, bf16[2048,512]{1,0:T(8,128)(2,1)} %param.23), kind=kOutput, calls=%fused_computation.20 | convolution fusion | flops 134250496 | bytes 2424832 | tf_op jit(solution)/shard_map/dot_general | solution.py:509
  2.8 0.1 reshape.101
  2.9 0.0 copy-start.2
  2.9 0.0 copy-start.3
  3.0 4.6 %fusion.2 = f32[64,8,1024]{2,1,0:T(8,128)S(1)} fusion(bf16[64,8,64]{2,1,0:T(8,128)(2,1)S(1)} %reshape.101, bf16[64,1,64,1024]{3,2,1,0:T(8,128)(2,1)} %param.20), kind=kOutput, calls=%fused_computation.2 | convolution fusion | flops 67108864 | bytes 10551296 | tf_op jit(solution)/shard_map/skgd,skdc->skgc/dot_general | solution.py:515
  7.5 0.0 copy-done.2
  7.5 0.1 iota_compare_fusion
  7.7 0.0 copy-done.3
  7.7 3.0 %fusion.32 = (f32[64,8,8]{1,2,0:T(8,128)S(1)}, f32[64,8,8,128]{3,1,2,0:T(8,128)}) fusion(f32[8]{0:T(128)S(1)} %copy-done.3, f32[64,8,1024]{2,1,0:T(8,128)S(1)} %fusion.2, pred[64,1024]{1,0:T(8,128)(4,1)S(1)} %iota_compare_fusion), kind=kLoop, calls=%fused_computation.37 | loop fusion | flops 5763072 | bytes 4276256 | tf_op jit(solution)/shard_map/reduce_sum | solution.py:38
  10.6 0.1 copy.32
  10.8 0.2 fusion.28
  10.9 0.1 copy.33
  11.1 4.2 %fusion.14 = f32[64,8,8,128]{3,2,1,0:T(8,128)} fusion(f32[64,8,8,128]{3,1,2,0:T(8,128)} %get-tuple-element.4, f32[64,8,8]{2,1,0:T(8,128)S(1)} %copy.33), kind=kOutput, calls=%fused_computation.18 | convolution fusion | flops 805847040 | bytes 4210688 | tf_op jit(solution)/shard_map/...bi,ic->...bc/dot_general | solution.py:35
  15.3 2.7 %reshape.104 = f32[64,8,1024]{2,1,0:T(8,128)} reshape(f32[64,8,8,128]{3,2,1,0:T(8,128)} %fusion.14) | data formatting | bytes 4194304 | tf_op jit(solution)/shard_map/reshape | solution.py:42
  18.0 6.4 %fusion.17 = bf16[64,8,64]{2,1,0:T(8,128)(2,1)S(1)} fusion(bf16[64,1,64,1024]{3,2,1,0:T(8,128)(2,1)} %param.21, f32[64,8,1024]{2,1,0:T(8,128)} %reshape.104, f32[64,8,1024]{2,1,0:T(8,128)S(1)} %fusion.2, f32[8]{0:T(128)S(1)} %copy-done.3, pred[64,1024]{1,0:T(8,128)(4,1)S(1)} %iota_compare_fusion), kind=kOutput, calls=%fused_computation.19 | convolution fusion | flops 73957376 | bytes 12714016 | tf_op jit(solution)/shard_map/skgc,skdc->skgd/dot_general | solution.py:525
  24.4 0.0 copy-start
  24.4 0.0 copy-start.1
  24.4 0.1 reshape.106
  24.5 2.8 %convolution_convert_fusion.part_ref = bf16[64,2048]{1,0:T(8,128)(2,1)} fusion(bf16[64,512]{1,0:T(8,128)(2,1)S(1)} %reshape.106, bf16[512,2048]{1,0:T(8,128)(2,1)} %param.27), kind=kOutput, calls=%fused_computation.6 | convolution fusion | flops 134348800 | bytes 2424832 | tf_op jit(solution)/shard_map/dot_general | solution.py:529
  27.3 0.0 copy-done
  27.3 0.3 copy.34
  27.6 0.9 pad.4.router_hbm
  28.5 0.0 copy-done.1
  28.5 0.7 convert_reduce_fusion.mask_ref
  29.2 66.8 %shard_map.202 = bf16[64,1024]{1,0:T(8,128)(2,1)} custom-call(bf16[64,2048]{1,0:T(8,128)(2,1)} %convolution_convert_fusion.part_ref, bf16[64,2048]{1,0:T(8,128)(2,1)} %inputs_ref.1, f32[64,128]{1,0:T(8,128)} %convert_reduce_fusion.mask_ref, f32[1,2048]{1,0:T(1,128)} %bitcast.39, f32[1,1024]{1,0:T(1,128)} %bitcast.40, bf16[2048,128]{1,0:T(8,128)(2,1)} %pad.4.router_hbm, ...), custom_call_target="tpu_custom_call" | custom-call | tf_op jit(solution)/shard_map/pallas_call | solution.py:434
  96.0 1.9 %convolution_convert_fusion.2 = bf16[64,64]{1,0:T(8,128)(2,1)} fusion(bf16[64,2048]{1,0:T(8,128)(2,1)} %inputs_ref.1, bf16[2048,64]{0,1:T(8,128)(2,1)} %param.25), kind=kOutput, calls=%fused_computation.21 | convolution fusion | flops 16781312 | bytes 532480 | tf_op jit(solution)/shard_map/dot_general | solution.py:512
  97.8 1.9 %convolution_convert_fusion.3 = bf16[64,64]{1,0:T(8,128)(2,1)} fusion(bf16[64,2048]{1,0:T(8,128)(2,1)} %inputs_ref.1, bf16[2048,64]{0,1:T(8,128)(2,1)} %param.24), kind=kOutput, calls=%fused_computation.22 | convolution fusion | flops 16781312 | bytes 532480 | tf_op jit(solution)/shard_map/dot_general | solution.py:511
  99.7 1.6 %copy.41 = bf16[64,1024]{1,0:T(8,128)(2,1)} copy(bf16[64,1024]{1,0:T(8,128)(2,1)} %shard_map.202) | data formatting | bytes 262144
Async XLA Ops:
  2.9 4.6 %copy-start.2 = (s32[64]{0:T(128)S(1)}, s32[64]{0:T(128)}, u32[]{:S(2)}) copy-start(s32[64]{0:T(128)} %param.22) | copy-start | bytes 772
  2.9 4.7 %copy-start.3 = (f32[8]{0:T(128)S(1)}, f32[8]{0:T(128)}, u32[]{:S(2)}) copy-start(f32[8]{0:T(128)} %param.26) | copy-start | bytes 100
  24.4 2.9 %copy-start = (bf16[2048,16]{0,1:T(8,128)(2,1)S(1)}, bf16[2048,16]{0,1:T(8,128)(2,1)}, u32[]{:S(2)}) copy-start(bf16[2048,16]{0,1:T(8,128)(2,1)} %param.29) | copy-start | bytes 196612
  24.4 4.1 %copy-start.1 = (s32[64,4]{0,1:T(4,128)S(1)}, s32[64,4]{0,1:T(4,128)}, u32[]{:S(2)}) copy-start(s32[64,4]{0,1:T(4,128)} %param.30) | copy-start | bytes 3076
